TPU v7x, 32 devices: a whole 2x2x4 slice. The times are simulated.
32 devices in a mesh: ep: 4 (over y, x), tp: 8 (over z, core).
Axes of the slice: x: 2, y: 2, z: 4, core: 2. Of those that a mesh axis runs over, the one named last changes fastest.
Arguments:
- query_rows: bfloat16 [512, 2048], P('ep', 'tp'), may hold values from -32 to 32
- key_rows: bfloat16 [512, 2048], P('ep', 'tp'), may hold values from -8 to 8
- value_rows: bfloat16 [512, 2048], P('ep', 'tp'), may hold values from -8 to 8
- query_norm_gain: float32 [64], replicated, may hold values from 0.1 to 1.9
- key_gain: float32 [64], replicated, may hold values from 0.1 to 1.9
- break_offset: float32 [32], P('tp'), may hold values from -12 to 3
- mixer_out_weight: bfloat16 [2048, 2048], P('tp'), may hold values from -0.75 to 0.75
- routed_tokens: bfloat16 [4096, 2048], P(('ep', 'tp')), may hold values from -6 to 6
- expert_gain: float32 [2048], replicated, may hold values from 0.1 to 1.9
- routes: int32 [4096, 2], P(('ep', 'tp')), may hold values from 0 to 3, as said below
- route_scores: float32 [4096, 2], P(('ep', 'tp')), may hold values from -6 to 6
- gate_weight: bfloat16 [4, 2048, 3584], P('ep', None, 'tp'), may hold values from -0.125 to 0.125
- up_weight: bfloat16 [4, 2048, 3584], P('ep', None, 'tp'), may hold values from -0.125 to 0.125
- down_weight: bfloat16 [4, 3584, 2048], P('ep', 'tp'), may hold values from -0.09375 to 0.09375
Outputs:
- attention_output: bfloat16 [512, 2048], P(('ep', 'tp'))
- expert_output: bfloat16 [4096, 2048], P(('ep', 'tp'))
Inputs may be any that keep to these rules, and one draw needn't show every extreme that they name: `routes`: each row names 2 different experts. Among the rows of one device no expert is named more than 64 times, and one expert is named exactly 64 times by the rows of every device.
All inputs are finite; a program needn't handle non-finite values.
Results may differ from a plain program's by a relative error of at most 0.018.
Values may be sent and summed in bfloat16 or wider, within the bound.
A program may use at most 128 MiB of HBM per device.

v0:
```python
import jax
import jax.numpy as jnp
from jax import lax
from jax.sharding import PartitionSpec as P

HEAD_DIM = 64
TOP_K = 2
EPS = 1e-06


def shifted(array, axis, by):
    peers = lax.axis_size(axis)
    pairs = [(i, i + by) for i in range(peers) if 0 <= i + by < peers]
    return lax.ppermute(array, axis, pairs)


def norm_heads(flat, gain):
    count = flat.shape[0]
    split = flat.astype(jnp.float32).reshape(count, -1, HEAD_DIM)
    scaled = split * lax.rsqrt(jnp.mean(split * split, axis=2, keepdims=True) + EPS)
    return (scaled * gain).astype(jnp.bfloat16)


def absorb(carry_state, query_norm, key_flat, value_flat, offsets, allowed):
    running_sum, carried = carry_state
    key_count = key_flat.shape[0]
    key_norm = key_flat.reshape(key_count, -1, HEAD_DIM)
    value_heads = value_flat.reshape(key_count, -1, HEAD_DIM)
    scores = jnp.einsum("qhd,khd->hqk", query_norm, key_norm, preferred_element_type=jnp.float32)
    scores = scores * HEAD_DIM ** (-0.5) + offsets[:, None, None]
    log_rise = jax.nn.log_sigmoid(scores)
    log_fail = jnp.where(allowed[None], log_rise - scores, 0.0)
    log_after = carried[:, :, None] + lax.cumsum(log_fail, axis=2, reverse=True) - log_fail
    weights = jnp.where(allowed[None], jnp.exp(log_rise + log_after), 0.0).astype(jnp.bfloat16)
    running_sum = running_sum + jnp.einsum(
        "hqk,khd->qhd", weights, value_heads, preferred_element_type=jnp.float32
    )
    return (running_sum, carried + jnp.sum(log_fail, axis=2))


def mixer_reduce(heads_mixed, mixer_out_weight):
    return lax.psum_scatter(
        jnp.dot(heads_mixed, mixer_out_weight, preferred_element_type=jnp.float32).astype(
            jnp.bfloat16
        ),
        "tp",
        scatter_dimension=0,
        tiled=True,
    ).astype(jnp.float32)


def body(
    query_rows,
    key_rows,
    value_rows,
    query_norm_gain,
    key_gain,
    break_offset,
    mixer_out_weight,
    routed_tokens,
    expert_gain,
    routes,
    route_scores,
    gate_weight,
    up_weight,
    down_weight,
):
    gate_local = gate_weight[0]
    up_local = up_weight[0]
    down_local = down_weight[0]
    row_count = query_rows.shape[0]
    query_norm = norm_heads(query_rows, query_norm_gain)
    head_count = query_norm.shape[1]
    key_flat = norm_heads(key_rows, key_gain).reshape(row_count, -1)
    my_index = lax.axis_index("ep")
    devices_ep = lax.axis_size("ep")
    token_position = jnp.arange(row_count)
    earlier = token_position[None, :] < token_position[:, None]
    carry_state = (
        jnp.zeros((row_count, head_count, HEAD_DIM), jnp.float32),
        jnp.zeros((head_count, row_count), jnp.float32),
    )
    carry_state = absorb(carry_state, query_norm, key_flat, value_rows, break_offset, earlier)

    def next_turn(turn_index, loop_carry):
        key_now, value_now, state_now = loop_carry
        key_now, value_now = shifted((key_now, value_now), "ep", 1)
        allowed = jnp.broadcast_to(my_index >= turn_index, (row_count, row_count))
        return (
            key_now,
            value_now,
            absorb(state_now, query_norm, key_now, value_now, break_offset, allowed),
        )

    carry_state = lax.fori_loop(1, devices_ep, next_turn, (key_flat, value_rows, carry_state))[2]
    heads_mixed = carry_state[0].astype(jnp.bfloat16).reshape(row_count, -1)
    token_count = routed_tokens.shape[0]
    model_width = routed_tokens.shape[1]
    as_float = routed_tokens.astype(jnp.float32)
    normed = (
        as_float
        * lax.rsqrt(jnp.mean(as_float * as_float, axis=1, keepdims=True) + EPS)
        * expert_gain
    ).astype(jnp.bfloat16)
    expert_count = lax.axis_size("ep")
    capacity = max(2, token_count * TOP_K // expert_count)
    flat_routes = routes.reshape(-1)
    member = (flat_routes[:, None] == jnp.arange(expert_count, dtype=jnp.int32)[None, :]).astype(
        jnp.int32
    )
    ahead = jnp.sum((jnp.cumsum(member, axis=0) - member) * member, axis=1)
    slot_index = flat_routes * capacity + ahead
    select = (
        slot_index[:, None] == jnp.arange(expert_count * capacity, dtype=jnp.int32)[None, :]
    ).astype(jnp.bfloat16)
    copies = jnp.repeat(normed, TOP_K, axis=0)
    outgoing = jnp.einsum("cs,cd->sd", select, copies, preferred_element_type=jnp.float32).astype(
        jnp.bfloat16
    )
    arrived = lax.all_to_all(outgoing, "ep", split_axis=0, concat_axis=0, tiled=True)
    piece = lax.all_gather(arrived, "tp", axis=0, tiled=True)
    gate_piece = jnp.dot(piece, gate_local, preferred_element_type=jnp.float32)
    up_piece = jnp.dot(piece, up_local, preferred_element_type=jnp.float32)
    hidden = (jax.nn.silu(gate_piece) * up_piece).astype(jnp.bfloat16)
    mixer_sum = mixer_reduce(heads_mixed, mixer_out_weight)
    expert_sum = lax.psum_scatter(
        jnp.dot(hidden, down_local, preferred_element_type=jnp.float32).astype(jnp.bfloat16),
        "tp",
        scatter_dimension=0,
        tiled=True,
    )
    returned = lax.all_to_all(expert_sum, "ep", split_axis=0, concat_axis=0, tiled=True)
    results = jnp.einsum("cs,sd->cd", select, returned, preferred_element_type=jnp.float32)
    results = results.reshape(token_count, TOP_K, model_width)
    differences = route_scores[:, None, :] - route_scores[:, :, None]
    route_weight = 1.0 / jnp.sum(jnp.exp(differences), axis=2)
    expert_output = jnp.sum(route_weight[..., None] * results, axis=1).astype(jnp.bfloat16)
    return (mixer_sum.astype(jnp.bfloat16), expert_output)


def solution(mesh):
    in_specs = (
        P("ep", "tp"),
        P("ep", "tp"),
        P("ep", "tp"),
        P(),
        P(),
        P("tp"),
        P("tp", None),
        P(("ep", "tp"), None),
        P(),
        P(("ep", "tp"), None),
        P(("ep", "tp"), None),
        P("ep", None, "tp"),
        P("ep", None, "tp"),
        P("ep", "tp", None),
    )
    out_specs = (P(("ep", "tp"), None), P(("ep", "tp"), None))
    return jax.shard_map(body, mesh=mesh, in_specs=in_specs, out_specs=out_specs, check_vma=False)
```

profile of v0, /device:TPU:0, one launch (start us, length us, event | category | flops | bytes accessed | tf_op | source)
XLA Modules:
  0.0 263.1 jit_solution(493648359935207742)
XLA Ops:
  7.2 0.0 copy-start
  7.2 0.0 all-gather.2.cloned.1.call-start
  7.2 0.9 copy.60
  8.1 0.1 eq.64
  8.3 0.1 eq.60
  8.4 1.2 reduce-window.6
  9.7 0.1 slice.8
  9.7 0.1 copy.62
  9.9 0.1 copy.63
  10.0 0.1 add_bitcast_fusion
  10.1 1.2 fusion.14
  11.3 1.2 fusion.16
  12.6 0.6 broadcast_in_dim.65
  13.2 1.2 reshape.147
  14.4 1.8 convolution_convert_fusion.1
  16.2 19.2 %all_to_all.24 = bf16[4,64,2048]{2,1,0:T(8,128)(2,1)} all-to-all(bf16[4,64,2048]{2,1,0:T(8,128)(2,1)S(1)} %bitcast.83), channel_id=1, replica_groups=mesh['ep'=4,'tp'=8] {'ep'}, dimensions={0} | all-to-all | bytes 2097152 | tf_op jit(solution)/shard_map/all_to_all | solution.py:120
  35.5 0.0 all-gather.2.cloned.1.call-update
  35.5 0.0 reduce-scatter.5.cloned.1.call-start
  35.5 81.9 %all-gather.2.cloned.1.call-done = bf16[2048,2048]{1,0:T(8,128)(2,1)} async-done(((bf16[256,2048]{1,0:T(8,128)(2,1)}), bf16[2048,2048]{1,0:T(8,128)(2,1)}) %all-gather.2.cloned.1.call-update) | async-done | bytes 8388624 | tf_op jit(solution)/shard_map/all_gather | solution.py:121
  117.4 7.2 %fusion.10 = f32[2048,448]{0,1:T(8,128)S(1)} fusion(bf16[2048,2048]{1,0:T(8,128)(2,1)} %all-gather.2.cloned.1.call-done, bf16[1,2048,448]{1,2,0:T(8,128)(2,1)} %param.27), kind=kOutput, calls=%fused_computation.22 | convolution fusion | flops 3758096384 | bytes 13893632 | tf_op jit(solution)/shard_map/dot_general | solution.py:122
  124.6 4.3 %multiply_convert_fusion = bf16[2048,448]{0,1:T(8,128)(2,1)S(1)} fusion(f32[2048,448]{0,1:T(8,128)S(1)} %fusion.10, bf16[2048,2048]{1,0:T(8,128)(2,1)S(1)} %copy-done.8, bf16[1,2048,448]{1,2,0:T(8,128)(2,1)S(1)} %copy-done.9), kind=kOutput, calls=%fused_computation.16 | convolution fusion | flops 3763601408 | bytes 15728640 | tf_op jit(solution)/shard_map/dot_general | solution.py:123
  128.9 6.9 %convolution_convert_fusion = bf16[2048,2048]{1,0:T(8,128)(2,1)} fusion(bf16[2048,448]{0,1:T(8,128)(2,1)S(1)} %multiply_convert_fusion, bf16[1,448,2048]{2,1,0:T(8,128)(2,1)S(1)} %copy-done), kind=kOutput, calls=%fused_computation.15 | convolution fusion | flops 3762290688 | bytes 12058624 | tf_op jit(solution)/shard_map/dot_general | solution.py:127
  135.8 0.0 reduce-scatter.5.cloned.1.call-update
  135.8 0.2 reduce-scatter.3.cloned.1.call-start
  136.1 0.5 copy-done.1
  136.6 0.1 copy.56
  136.7 0.1 copy.55
  136.9 0.1 copy.59
  137.0 0.1 mul.119
  137.1 0.1 fusion.20
  137.3 0.1 multiply_convert_fusion.2
  137.4 0.3 fusion.26
  137.7 0.2 fusion.33
  138.0 4.4 %reduce_window_sum.35 = f32[4,128,128]{1,2,0:T(8,128)S(1)} reduce-window(f32[4,128,128]{1,2,0:T(8,128)S(1)} %get-tuple-element.197, f32[]{:T(128)} %constant.53.clone.1), window={size=1x1x128 pad=0_0x0_0x0_127}, to_apply=%region_2.3 | reduce-window | flops 8323072 | bytes 524292 | tf_op jit(solution)/shard_map/absorb/reduce_window_sum | solution.py:33
  142.4 0.4 convolution_bitcast_fusion.1
  142.8 36.9 %while.19 = (s32[]{:T(128)}, bf16[128,256]{0,1:T(8,128)(2,1)S(1)}, bf16[128,256]{0,1:T(8,128)(2,1)S(1)}, f32[128,4,64]{0,2,1:T(8,128)S(1)}, f32[4,128]{1,0:T(4,1...) while((s32[]{:T(128)}, bf16[128,256]{0,1:T(8,128)(2,1)S(1)}, ...), condition=%wide.region_7.8_spmd, body=%wide.region_4.7_spmd.sunk | while | flops 27738116 | bytes 3139796 | solution.py:95
  142.8 3.4 %collective-permute-start = (bf16[128,256]{0,1:T(8,128)(2,1)S(1)}, bf16[128,256]{0,1:T(8,128)(2,1)S(1)}, u32[]{:S(2)}, u32[]{:S(2)}) collective-permute-start(bf16[128,256]{0,1:T(8,128)(2,1)S(1)} %get-tuple-element.268), channel_id=1, source_target_pairs={{0,8},{8,16},{16,24},{1,9},{9,17},{17,25},{2,10},{10,18},{18,26},{... | collective-permute-start | bytes 196616 | tf_op jit(solution)/shard_map/while/body/eval_jaxpr/ppermute | solution.py:14
  146.1 3.4 %collective-permute-start.1 = (bf16[128,256]{0,1:T(8,128)(2,1)S(1)}, bf16[128,256]{0,1:T(8,128)(2,1)S(1)}, u32[]{:S(2)}, u32[]{:S(2)}) collective-permute-start(bf16[128,256]{0,1:T(8,128)(2,1)S(1)} %get-tuple-element.269), channel_id=1, source_target_pairs={{0,8},{8,16},{16,24},{1,9},{9,17},{17,25},{2,10},{10,18},{18,26},{... | collective-permute-start | bytes 196616 | tf_op jit(solution)/shard_map/while/body/eval_jaxpr/ppermute | solution.py:14
  149.5 0.3 fusion.55
  149.8 0.2 fusion.56
  150.0 4.4 %reduce_window_sum.40 = f32[4,128,128]{1,2,0:T(8,128)S(1)} reduce-window(f32[4,128,128]{1,2,0:T(8,128)S(1)} %get-tuple-element.255, f32[]{:T(128)} %constant.53.clone.1..sunk), window={size=1x1x128 pad=0_0x0_0x0_127}, to_apply=%region_5.5 | reduce-window | flops 8323072 | bytes 524292 | tf_op jit(solution)/shard_map/while/body/eval_jaxpr/reduce_window_sum | solution.py:33
  154.5 0.4 fusion.57
  154.9 3.4 %collective-permute-start = (bf16[128,256]{0,1:T(8,128)(2,1)S(1)}, bf16[128,256]{0,1:T(8,128)(2,1)S(1)}, u32[]{:S(2)}, u32[]{:S(2)}) collective-permute-start(bf16[128,256]{0,1:T(8,128)(2,1)S(1)} %get-tuple-element.268), channel_id=1, source_target_pairs={{0,8},{8,16},{16,24},{1,9},{9,17},{17,25},{2,10},{10,18},{18,26},{... | collective-permute-start | bytes 196616 | tf_op jit(solution)/shard_map/while/body/eval_jaxpr/ppermute | solution.py:14
  158.3 3.6 %collective-permute-start.1 = (bf16[128,256]{0,1:T(8,128)(2,1)S(1)}, bf16[128,256]{0,1:T(8,128)(2,1)S(1)}, u32[]{:S(2)}, u32[]{:S(2)}) collective-permute-start(bf16[128,256]{0,1:T(8,128)(2,1)S(1)} %get-tuple-element.269), channel_id=1, source_target_pairs={{0,8},{8,16},{16,24},{1,9},{9,17},{17,25},{2,10},{10,18},{18,26},{... | collective-permute-start | bytes 196616 | tf_op jit(solution)/shard_map/while/body/eval_jaxpr/ppermute | solution.py:14
  161.9 0.3 fusion.55
  162.2 0.2 fusion.56
  162.4 4.4 %reduce_window_sum.40 = f32[4,128,128]{1,2,0:T(8,128)S(1)} reduce-window(f32[4,128,128]{1,2,0:T(8,128)S(1)} %get-tuple-element.255, f32[]{:T(128)} %constant.53.clone.1..sunk), window={size=1x1x128 pad=0_0x0_0x0_127}, to_apply=%region_5.5 | reduce-window | flops 8323072 | bytes 524292 | tf_op jit(solution)/shard_map/while/body/eval_jaxpr/reduce_window_sum | solution.py:33
  166.9 0.4 fusion.57
  167.3 2.5 collective-permute-start
  169.8 4.5 %collective-permute-start.1 = (bf16[128,256]{0,1:T(8,128)(2,1)S(1)}, bf16[128,256]{0,1:T(8,128)(2,1)S(1)}, u32[]{:S(2)}, u32[]{:S(2)}) collective-permute-start(bf16[128,256]{0,1:T(8,128)(2,1)S(1)} %get-tuple-element.269), channel_id=1, source_target_pairs={{0,8},{8,16},{16,24},{1,9},{9,17},{17,25},{2,10},{10,18},{18,26},{... | collective-permute-start | bytes 196616 | tf_op jit(solution)/shard_map/while/body/eval_jaxpr/ppermute | solution.py:14
  174.4 0.3 fusion.55
  174.6 0.2 fusion.56
  174.8 4.4 %reduce_window_sum.40 = f32[4,128,128]{1,2,0:T(8,128)S(1)} reduce-window(f32[4,128,128]{1,2,0:T(8,128)S(1)} %get-tuple-element.255, f32[]{:T(128)} %constant.53.clone.1..sunk), window={size=1x1x128 pad=0_0x0_0x0_127}, to_apply=%region_5.5 | reduce-window | flops 8323072 | bytes 524292 | tf_op jit(solution)/shard_map/while/body/eval_jaxpr/reduce_window_sum | solution.py:33
  179.3 0.4 fusion.57
  179.7 0.0 copy-start.4
  179.8 2.4 convolution_convert_fusion.2
  182.1 0.0 reduce-scatter.3.cloned.1.call-update
  182.1 41.8 %reduce-scatter.5.cloned.1.call-done = bf16[256,2048]{1,0:T(8,128)(2,1)} async-done(((bf16[2048,2048]{1,0:T(8,128)(2,1)}), bf16[256,2048]{1,0:T(8,128)(2,1)}) %reduce-scatter.5.cloned.1.call-update) | async-done | bytes 1048592 | tf_op jit(solution)/shard_map/reduce_scatter | solution.py:126
  223.9 3.7 %all-to-all-start.1 = ((bf16[4,64,2048]{2,1,0:T(8,128)(2,1)}), bf16[4,64,2048]{2,1,0:T(8,128)(2,1)S(1)}, u32[]{:S(2)}, u32[]{:S(2)}) async-start(bf16[4,64,2048]{2,1,0:T(8,128)(2,1)} %bitcast.86), calls=%async_computation.3 | async-start | bytes 2097152 | tf_op jit(solution)/shard_map/all_to_all | solution.py:132
  227.7 0.1 reduce_sum.83
  227.8 0.1 copy.64
  227.9 11.7 %all-to-all-done.1 = bf16[4,64,2048]{2,1,0:T(8,128)(2,1)S(1)} async-done(((bf16[4,64,2048]{2,1,0:T(8,128)(2,1)}), bf16[4,64,2048]{2,1,0:T(8,128)(2,1)S(1)}, u32[]{:S(2)}, u32[]{:S(2)}) %all-to-all-start.1) | async-done | bytes 1048608 | tf_op jit(solution)/shard_map/all_to_all | solution.py:132
  239.6 1.3 fusion.12
  241.0 15.6 %reduce-scatter.3.cloned.1.call-done = bf16[16,2048]{1,0:T(8,128)(2,1)} async-done(((bf16[128,2048]{1,0:T(8,128)(2,1)}), bf16[16,2048]{1,0:T(8,128)(2,1)}) %reduce-scatter.3.cloned.1.call-update) | async-done | bytes 65552 | tf_op jit(solution)/shard_map/reduce_scatter | solution.py:42
  (50 shorter events, 0.4 us)
Async XLA Ops:
  7.2 121.7 %copy-start = (bf16[1,448,2048]{2,1,0:T(8,128)(2,1)S(1)}, bf16[1,448,2048]{2,1,0:T(8,128)(2,1)}, u32[]{:S(2)}) copy-start(bf16[1,448,2048]{2,1,0:T(8,128)(2,1)} %param.29) | copy-start | bytes 5505028
  7.2 110.2 %all-gather.2.cloned.1.call-start = ((), (), s32[]{:S(2)}) async-start(), calls=%async_computation.5 | async-start | bytes 9437184 | tf_op jit(solution)/shard_map/all_gather | solution.py:121
  35.5 188.5 %reduce-scatter.5.cloned.1.call-start = ((), (), s32[]{:S(2)}) async-start(), calls=%async_computation.6 | async-start | bytes 9437184 | tf_op jit(solution)/shard_map/reduce_scatter | solution.py:126
  117.4 7.2 %copy-start.8 = (bf16[2048,2048]{1,0:T(8,128)(2,1)S(1)}, bf16[2048,2048]{1,0:T(8,128)(2,1)}, u32[]{:S(2)}) copy-start(bf16[2048,2048]{1,0:T(8,128)(2,1)} %all-gather.2.cloned.1.call-done) | copy-start | bytes 25165828
  117.4 7.2 %copy-start.9 = (bf16[1,2048,448]{1,2,0:T(8,128)(2,1)S(1)}, bf16[1,2048,448]{1,2,0:T(8,128)(2,1)}, u32[]{:S(2)}) copy-start(bf16[1,2048,448]{1,2,0:T(8,128)(2,1)} %param.28) | copy-start | bytes 5505028
  135.8 0.8 copy-start.1
  135.8 0.9 copy-start.2
  135.8 1.1 copy-start.3
  135.8 1.2 copy-start.7
  135.8 1.5 copy-start.6
  135.8 1.6 copy-start.10
  135.8 120.7 %reduce-scatter.3.cloned.1.call-start = ((), (), s32[]{:S(2)}) async-start(), calls=%async_computation.4 | async-start | bytes 589824 | tf_op jit(solution)/shard_map/reduce_scatter | solution.py:42
  142.8 6.8 %collective-permute-start = (bf16[128,256]{0,1:T(8,128)(2,1)S(1)}, bf16[128,256]{0,1:T(8,128)(2,1)S(1)}, u32[]{:S(2)}, u32[]{:S(2)}) collective-permute-start(bf16[128,256]{0,1:T(8,128)(2,1)S(1)} %get-tuple-element.268), channel_id=1, source_target_pairs={{0,8},{8,16},{16,24},{1,9},{9,17},{17,25},{2,10},{10,18},{18,26},{... | collective-permute-start | bytes 196616 | tf_op jit(solution)/shard_map/while/body/eval_jaxpr/ppermute | solution.py:14
  146.1 8.3 %collective-permute-start.1 = (bf16[128,256]{0,1:T(8,128)(2,1)S(1)}, bf16[128,256]{0,1:T(8,128)(2,1)S(1)}, u32[]{:S(2)}, u32[]{:S(2)}) collective-permute-start(bf16[128,256]{0,1:T(8,128)(2,1)S(1)} %get-tuple-element.269), channel_id=1, source_target_pairs={{0,8},{8,16},{16,24},{1,9},{9,17},{17,25},{2,10},{10,18},{18,26},{... | collective-permute-start | bytes 196616 | tf_op jit(solution)/shard_map/while/body/eval_jaxpr/ppermute | solution.py:14
  154.9 7.0 %collective-permute-start = (bf16[128,256]{0,1:T(8,128)(2,1)S(1)}, bf16[128,256]{0,1:T(8,128)(2,1)S(1)}, u32[]{:S(2)}, u32[]{:S(2)}) collective-permute-start(bf16[128,256]{0,1:T(8,128)(2,1)S(1)} %get-tuple-element.268), channel_id=1, source_target_pairs={{0,8},{8,16},{16,24},{1,9},{9,17},{17,25},{2,10},{10,18},{18,26},{... | collective-permute-start | bytes 196616 | tf_op jit(solution)/shard_map/while/body/eval_jaxpr/ppermute | solution.py:14
  158.3 8.6 %collective-permute-start.1 = (bf16[128,256]{0,1:T(8,128)(2,1)S(1)}, bf16[128,256]{0,1:T(8,128)(2,1)S(1)}, u32[]{:S(2)}, u32[]{:S(2)}) collective-permute-start(bf16[128,256]{0,1:T(8,128)(2,1)S(1)} %get-tuple-element.269), channel_id=1, source_target_pairs={{0,8},{8,16},{16,24},{1,9},{9,17},{17,25},{2,10},{10,18},{18,26},{... | collective-permute-start | bytes 196616 | tf_op jit(solution)/shard_map/while/body/eval_jaxpr/ppermute | solution.py:14
  167.3 7.0 %collective-permute-start = (bf16[128,256]{0,1:T(8,128)(2,1)S(1)}, bf16[128,256]{0,1:T(8,128)(2,1)S(1)}, u32[]{:S(2)}, u32[]{:S(2)}) collective-permute-start(bf16[128,256]{0,1:T(8,128)(2,1)S(1)} %get-tuple-element.268), channel_id=1, source_target_pairs={{0,8},{8,16},{16,24},{1,9},{9,17},{17,25},{2,10},{10,18},{18,26},{... | collective-permute-start | bytes 196616 | tf_op jit(solution)/shard_map/while/body/eval_jaxpr/ppermute | solution.py:14
  169.8 9.5 %collective-permute-start.1 = (bf16[128,256]{0,1:T(8,128)(2,1)S(1)}, bf16[128,256]{0,1:T(8,128)(2,1)S(1)}, u32[]{:S(2)}, u32[]{:S(2)}) collective-permute-start(bf16[128,256]{0,1:T(8,128)(2,1)S(1)} %get-tuple-element.269), channel_id=1, source_target_pairs={{0,8},{8,16},{16,24},{1,9},{9,17},{17,25},{2,10},{10,18},{18,26},{... | collective-permute-start | bytes 196616 | tf_op jit(solution)/shard_map/while/body/eval_jaxpr/ppermute | solution.py:14
  179.7 48.2 %copy-start.5 = (f32[128,2]{0,1:T(2,128)S(1)}, f32[128,2]{0,1:T(2,128)}, u32[]{:S(2)}) copy-start(f32[128,2]{0,1:T(2,128)} %param.26) | copy-start | bytes 3076
  179.7 48.2 %copy-start.4 = (s32[128,2]{0,1:T(2,128)S(1)}, s32[128,2]{0,1:T(2,128)}, u32[]{:S(2)}) copy-start(s32[128,2]{0,1:T(2,128)} %param.25) | copy-start | bytes 3076
  223.9 15.7 %all-to-all-start.1 = ((bf16[4,64,2048]{2,1,0:T(8,128)(2,1)}), bf16[4,64,2048]{2,1,0:T(8,128)(2,1)S(1)}, u32[]{:S(2)}, u32[]{:S(2)}) async-start(bf16[4,64,2048]{2,1,0:T(8,128)(2,1)} %bitcast.86), calls=%async_computation.3 | async-start | bytes 2097152 | tf_op jit(solution)/shard_map/all_to_all | solution.py:132
Sparse Core Ops, SparseCore 0:
  35.6 81.7 all-gather.1
  136.0 87.9 reduce-scatter.4
  226.8 29.7 reduce-scatter.2
where the time goes:
time: 264 us; the launch traced here: 263 us
  waiting for transfers between devices  151 us (57%)
  matrix products  26.4 us (10%)
  starting transfers between devices  24.8 us (9%)
  other arithmetic  22.8 us (9%)
  blocking collectives  19.2 us (7%)
  between operations  14 us (5%)
  local copies, waits for them, and re-layouts  4.56 us (2%)
    all_gather x1, waiting for transfers between devices, body(): piece = lax.all_gather(arrived, 'tp', axis=0, tiled=True)  81.9 us
    reduce_scatter x1, waiting for transfers between devices, body(): lax.psum_scatter(jnp.dot(hidden, down_local, preferred_element_type=jnp.f...  41.8 us
    ppermute x6, starting transfers between devices, shifted(): return lax.ppermute(array, axis, pairs)  20.8 us
    all_to_all x1, blocking collectives, body(): lax.all_to_all(outgoing, 'ep', split_axis=0, concat_axis=0, tiled=True)  19.2 us
    another operation x4, other arithmetic, absorb(): lax.cumsum(log_fail, axis=2, reverse=True)  17.7 us
    reduce_scatter x1, waiting for transfers between devices, mixer_reduce(): lax.psum_scatter(jnp.dot(heads_mixed, mixer_out_weight, preferred_element...  15.6 us
    all_to_all x1, waiting for transfers between devices, body(): lax.all_to_all(expert_sum, 'ep', split_axis=0, concat_axis=0, tiled=True)  11.7 us
    dot_general x1, matrix products, body(): gate_piece = jnp.dot(piece, gate_local, preferred_element_type=jnp.float32)  7.17 us
  transfers between devices with their start and end apart: 10, of which 4 were waited for; matrix products, arithmetic and copies ran while one was open for 10% of the time, Pallas kernels for 0%

commit v1 on v0

--- a/solution.py
+++ b/solution.py
@@ -118,7 +118,19 @@
         jnp.bfloat16
     )
     arrived = lax.all_to_all(outgoing, "ep", split_axis=0, concat_axis=0, tiled=True)
-    piece = lax.all_gather(arrived, "tp", axis=0, tiled=True)
+
+    def trace_results(mesh_dim, u):
+        devs = lax.psum(1, axis_name=mesh_dim)
+        all_rows = [None] * devs
+        buffer = [(kk, (kk + 1) % devs) for kk in range(devs)]
+        all_rows[devs - 1] = u
+        for j0 in range(devs - 2, -1, -1):
+            all_rows[j0] = lax.ppermute(all_rows[j0 + 1], axis_name=mesh_dim, perm=buffer)
+        t1 = jnp.concatenate(all_rows, axis=0)
+        s_next = (lax.axis_index(mesh_dim) + 1) * u.shape[0]
+        return jnp.roll(t1, shift=s_next, axis=0)
+
+    piece = trace_results("tp", u=arrived)
     gate_piece = jnp.dot(piece, gate_local, preferred_element_type=jnp.float32)
     up_piece = jnp.dot(piece, up_local, preferred_element_type=jnp.float32)
     hidden = (jax.nn.silu(gate_piece) * up_piece).astype(jnp.bfloat16)

time: 264 us -> 318 us (1.20)
  waiting for transfers between devices: 151 us -> 181 us
  local copies, waits for them, and re-layouts: 4.56 us -> 26.8 us
    ppermute x0 -> x7, waiting for transfers between devices: none -> 113 us  [trace_results(): lax.ppermute(all_rows[j0 + 1], axis_name=mesh_dim, perm=buffer)]
    all_gather x1 -> x0, waiting for transfers between devices: 81.9 us -> none  [body(): piece = lax.all_gather(arrived, 'tp', axis=0, tiled=True)]
    unnamed x24 -> x59, local copies, waits for them, and re-layouts: 1.62 us -> 23.8 us
    dot_general x1, matrix products: 6.89 us -> 14.3 us  [body(): jnp.dot(hidden, down_local, preferred_element_type=jnp.float32)]
    dot_general x1 -> x0, matrix products: 7.17 us -> none  [body(): gate_piece = jnp.dot(piece, gate_local, preferred_element_type=jnp.float32)]
  transfers between devices with their start and end apart: 10 -> 16, of which waited for: 4 -> 10; matrix products, arithmetic and copies ran while one was open for 10% -> 8% of each run, Pallas kernels for 0% -> 0%
where the time goes in v1:
time: 318 us; the launch traced here: 317 us
  waiting for transfers between devices  181 us (57%)
  matrix products  28.3 us (9%)
  local copies, waits for them, and re-layouts  26.8 us (8%)
  starting transfers between devices  24.2 us (8%)
  other arithmetic  22.8 us (7%)
  blocking collectives  19.1 us (6%)
  between operations  14.5 us (5%)
    ppermute x7, waiting for transfers between devices, trace_results(): lax.ppermute(all_rows[j0 + 1], axis_name=mesh_dim, perm=buffer)  113 us
    reduce_scatter x1, waiting for transfers between devices, body(): lax.psum_scatter(jnp.dot(hidden, down_local, preferred_element_type=jnp.f...  41.1 us
    unnamed x59, local copies, waits for them, and re-layouts  23.8 us
    ppermute x6, starting transfers between devices, shifted(): return lax.ppermute(array, axis, pairs)  20.2 us
    all_to_all x1, blocking collectives, body(): lax.all_to_all(outgoing, 'ep', split_axis=0, concat_axis=0, tiled=True)  19.1 us
    another operation x4, other arithmetic, absorb(): lax.cumsum(log_fail, axis=2, reverse=True)  17.7 us
    reduce_scatter x1, waiting for transfers between devices, mixer_reduce(): lax.psum_scatter(jnp.dot(heads_mixed, mixer_out_weight, preferred_element...  15.9 us
    dot_general x1, matrix products, body(): jnp.dot(hidden, down_local, preferred_element_type=jnp.float32)  14.3 us
  transfers between devices with their start and end apart: 16, of which 10 were waited for; matrix products, arithmetic and copies ran while one was open for 8% of the time, Pallas kernels for 0%

profile of v1, /device:TPU:0, one launch (start us, length us, event | category | flops | bytes accessed | tf_op | source)
XLA Modules:
  0.0 317.1 jit_solution(951845238459855287)
XLA Ops:
  7.2 0.9 copy.60
  8.1 0.1 eq.67
  8.3 0.1 eq.63
  8.4 1.2 reduce-window.6
  10.1 1.2 fusion.23
  11.3 1.2 fusion.25
  12.6 0.6 broadcast_in_dim.65
  13.2 1.2 reshape.147
  14.4 1.8 convolution_convert_fusion.1
  16.2 19.1 %all_to_all.24 = bf16[4,64,2048]{2,1,0:T(8,128)(2,1)S(1)} all-to-all(bf16[4,64,2048]{2,1,0:T(8,128)(2,1)S(1)} %bitcast.83), channel_id=1, replica_groups=mesh['ep'=4,'tp'=8] {'ep'}, dimensions={0} | all-to-all | bytes 2097152 | tf_op jit(solution)/shard_map/all_to_all | solution.py:120
  35.4 16.0 %collective-permute-done.2 = bf16[256,2048]{1,0:T(8,128)(2,1)S(1)} collective-permute-done((bf16[256,2048]{1,0:T(8,128)(2,1)S(1)}, bf16[256,2048]{1,0:T(8,128)(2,1)S(1)}, u32[]{:S(2)}, u32[]{:S(2)}) %collective-permute-start.2) | collective-permute-done | bytes 1048608 | tf_op jit(solution)/shard_map/ppermute | solution.py:128
  51.4 1.0 copy-done.1
  52.4 16.0 %collective-permute-done.3 = bf16[256,2048]{1,0:T(8,128)(2,1)S(1)} collective-permute-done((bf16[256,2048]{1,0:T(8,128)(2,1)S(1)}, bf16[256,2048]{1,0:T(8,128)(2,1)S(1)}, u32[]{:S(2)}, u32[]{:S(2)}) %collective-permute-start.3) | collective-permute-done | bytes 1048608 | tf_op jit(solution)/shard_map/ppermute | solution.py:128
  68.4 1.0 copy-done.3
  69.4 16.0 %collective-permute-done.4 = bf16[256,2048]{1,0:T(8,128)(2,1)S(1)} collective-permute-done((bf16[256,2048]{1,0:T(8,128)(2,1)S(1)}, bf16[256,2048]{1,0:T(8,128)(2,1)S(1)}, u32[]{:S(2)}, u32[]{:S(2)}) %collective-permute-start.4) | collective-permute-done | bytes 1048608 | tf_op jit(solution)/shard_map/ppermute | solution.py:128
  85.4 1.0 copy-done.5
  86.4 16.0 %collective-permute-done.5 = bf16[256,2048]{1,0:T(8,128)(2,1)S(1)} collective-permute-done((bf16[256,2048]{1,0:T(8,128)(2,1)S(1)}, bf16[256,2048]{1,0:T(8,128)(2,1)S(1)}, u32[]{:S(2)}, u32[]{:S(2)}) %collective-permute-start.5) | collective-permute-done | bytes 1048608 | tf_op jit(solution)/shard_map/ppermute | solution.py:128
  102.5 1.0 copy-done.7
  103.4 16.0 %collective-permute-done.6 = bf16[256,2048]{1,0:T(8,128)(2,1)S(1)} collective-permute-done((bf16[256,2048]{1,0:T(8,128)(2,1)S(1)}, bf16[256,2048]{1,0:T(8,128)(2,1)S(1)}, u32[]{:S(2)}, u32[]{:S(2)}) %collective-permute-start.6) | collective-permute-done | bytes 1048608 | tf_op jit(solution)/shard_map/ppermute | solution.py:128
  119.5 1.0 copy-done.9
  120.4 16.1 %collective-permute-done.7 = bf16[256,2048]{1,0:T(8,128)(2,1)} collective-permute-done((bf16[256,2048]{1,0:T(8,128)(2,1)S(1)}, bf16[256,2048]{1,0:T(8,128)(2,1)}, u32[]{:S(2)}, u32[]{:S(2)}) %collective-permute-start.7) | collective-permute-done | bytes 1048608 | tf_op jit(solution)/shard_map/ppermute | solution.py:128
  136.6 16.3 %collective-permute-done.8 = bf16[256,2048]{1,0:T(8,128)(2,1)} collective-permute-done((bf16[256,2048]{1,0:T(8,128)(2,1)}, bf16[256,2048]{1,0:T(8,128)(2,1)}, u32[]{:S(2)}, u32[]{:S(2)}) %collective-permute-start.8) | collective-permute-done | bytes 1048608 | tf_op jit(solution)/shard_map/ppermute | solution.py:128
  152.9 1.3 constant_dynamic-update-slice_fusion.15
  154.2 1.3 constant_dynamic-update-slice_fusion.14
  155.5 1.3 constant_dynamic-update-slice_fusion.13
  156.8 1.3 constant_dynamic-update-slice_fusion.12
  158.1 1.3 constant_dynamic-update-slice_fusion.11
  159.4 1.3 constant_dynamic-update-slice_fusion.10
  160.7 1.3 constant_dynamic-update-slice_fusion.9
  162.1 1.3 constant_dynamic-update-slice_fusion.7
  163.4 1.3 constant_dynamic-update-slice_fusion.6
  165.2 5.7 %copy-done.12 = bf16[4096,2048]{1,0:T(8,128)(2,1)} copy-done((bf16[4096,2048]{1,0:T(8,128)(2,1)}, bf16[4096,2048]{1,0:T(8,128)(2,1)S(1)}, u32[]{:S(2)}) %copy-start.12) | copy-done | bytes 16777240
  170.9 5.9 %fusion.8 = f32[2048,448]{0,1:T(8,128)} fusion(bf16[4096,2048]{1,0:T(8,128)(2,1)S(1)} %constant_dynamic-update-slice_fusion, s32[]{:T(128)S(6)} %select_n.50, bf16[1,2048,448]{1,2,0:T(8,128)(2,1)S(1)} %copy-done.19), kind=kOutput, calls=%fused_computation.16 | convolution fusion | flops 3758096384 | bytes 13893636 | tf_op jit(solution)/shard_map/dot_general | solution.py:135
  176.8 14.3 %convolution_convert_fusion = bf16[2048,2048]{1,0:T(8,128)(2,1)} fusion(f32[2048,448]{0,1:T(8,128)} %fusion.8, bf16[1,448,2048]{2,1,0:T(8,128)(2,1)S(1)} %copy-done, bf16[4096,2048]{1,0:T(8,128)(2,1)} %copy-done.12, s32[]{:T(128)S(6)} %select_n.50, bf16[1,2048,448]{1,2,0:T(8,128)(2,1)} %param.27), kind=kOutput, calls=%fused_computation.15 | convolution fusion | flops 7525892096 | bytes 24117252 | tf_op jit(solution)/shard_map/dot_general | solution.py:139
  191.2 0.3 reduce-scatter.3.cloned.1.call-start
  192.2 0.3 fusion.35
  192.6 0.2 fusion.46
  192.8 4.4 %reduce_window_sum.35 = f32[4,128,128]{1,2,0:T(8,128)S(1)} reduce-window(f32[4,128,128]{1,2,0:T(8,128)S(1)} %get-tuple-element.197, f32[]{:T(128)} %constant.74.clone.1), window={size=1x1x128 pad=0_0x0_0x0_127}, to_apply=%region_2.3 | reduce-window | flops 8323072 | bytes 524292 | tf_op jit(solution)/shard_map/absorb/reduce_window_sum | solution.py:33
  197.2 0.4 convolution_bitcast_fusion.1
  197.6 36.4 %while.19 = (s32[]{:T(128)}, bf16[128,256]{0,1:T(8,128)(2,1)S(1)}, bf16[128,256]{0,1:T(8,128)(2,1)S(1)}, f32[128,4,64]{0,2,1:T(8,128)S(1)}, f32[4,128]{1,0:T(4,1...) while((s32[]{:T(128)}, bf16[128,256]{0,1:T(8,128)(2,1)S(1)}, ...), condition=%wide.region_7.8_spmd, body=%wide.region_4.7_spmd.sunk | while | flops 27738116 | bytes 3139796 | solution.py:95
  197.6 2.8 collective-permute-start
  200.4 3.4 %collective-permute-start.1 = (bf16[128,256]{0,1:T(8,128)(2,1)S(1)}, bf16[128,256]{0,1:T(8,128)(2,1)S(1)}, u32[]{:S(2)}, u32[]{:S(2)}) collective-permute-start(bf16[128,256]{0,1:T(8,128)(2,1)S(1)} %get-tuple-element.269), channel_id=1, source_target_pairs={{0,8},{8,16},{16,24},{1,9},{9,17},{17,25},{2,10},{10,18},{18,26},{... | collective-permute-start | bytes 196616 | tf_op jit(solution)/shard_map/while/body/eval_jaxpr/ppermute | solution.py:14
  203.8 0.3 fusion.65
  204.1 0.2 fusion.66
  204.3 4.4 %reduce_window_sum.40 = f32[4,128,128]{1,2,0:T(8,128)S(1)} reduce-window(f32[4,128,128]{1,2,0:T(8,128)S(1)} %get-tuple-element.255, f32[]{:T(128)} %constant.74.clone.1..sunk), window={size=1x1x128 pad=0_0x0_0x0_127}, to_apply=%region_5.5 | reduce-window | flops 8323072 | bytes 524292 | tf_op jit(solution)/shard_map/while/body/eval_jaxpr/reduce_window_sum | solution.py:33
  208.7 0.4 fusion.67
  209.2 3.4 %collective-permute-start = (bf16[128,256]{0,1:T(8,128)(2,1)S(1)}, bf16[128,256]{0,1:T(8,128)(2,1)S(1)}, u32[]{:S(2)}, u32[]{:S(2)}) collective-permute-start(bf16[128,256]{0,1:T(8,128)(2,1)S(1)} %get-tuple-element.268), channel_id=1, source_target_pairs={{0,8},{8,16},{16,24},{1,9},{9,17},{17,25},{2,10},{10,18},{18,26},{... | collective-permute-start | bytes 196616 | tf_op jit(solution)/shard_map/while/body/eval_jaxpr/ppermute | solution.py:14
  212.6 3.6 %collective-permute-start.1 = (bf16[128,256]{0,1:T(8,128)(2,1)S(1)}, bf16[128,256]{0,1:T(8,128)(2,1)S(1)}, u32[]{:S(2)}, u32[]{:S(2)}) collective-permute-start(bf16[128,256]{0,1:T(8,128)(2,1)S(1)} %get-tuple-element.269), channel_id=1, source_target_pairs={{0,8},{8,16},{16,24},{1,9},{9,17},{17,25},{2,10},{10,18},{18,26},{... | collective-permute-start | bytes 196616 | tf_op jit(solution)/shard_map/while/body/eval_jaxpr/ppermute | solution.py:14
  216.2 0.3 fusion.65
  216.5 0.2 fusion.66
  216.7 4.4 %reduce_window_sum.40 = f32[4,128,128]{1,2,0:T(8,128)S(1)} reduce-window(f32[4,128,128]{1,2,0:T(8,128)S(1)} %get-tuple-element.255, f32[]{:T(128)} %constant.74.clone.1..sunk), window={size=1x1x128 pad=0_0x0_0x0_127}, to_apply=%region_5.5 | reduce-window | flops 8323072 | bytes 524292 | tf_op jit(solution)/shard_map/while/body/eval_jaxpr/reduce_window_sum | solution.py:33
  221.1 0.4 fusion.67
  221.6 2.8 collective-permute-start
  224.3 4.3 %collective-permute-start.1 = (bf16[128,256]{0,1:T(8,128)(2,1)S(1)}, bf16[128,256]{0,1:T(8,128)(2,1)S(1)}, u32[]{:S(2)}, u32[]{:S(2)}) collective-permute-start(bf16[128,256]{0,1:T(8,128)(2,1)S(1)} %get-tuple-element.269), channel_id=1, source_target_pairs={{0,8},{8,16},{16,24},{1,9},{9,17},{17,25},{2,10},{10,18},{18,26},{... | collective-permute-start | bytes 196616 | tf_op jit(solution)/shard_map/while/body/eval_jaxpr/ppermute | solution.py:14
  228.6 0.3 fusion.65
  228.9 0.2 fusion.66
  229.1 4.4 %reduce_window_sum.40 = f32[4,128,128]{1,2,0:T(8,128)S(1)} reduce-window(f32[4,128,128]{1,2,0:T(8,128)S(1)} %get-tuple-element.255, f32[]{:T(128)} %constant.74.clone.1..sunk), window={size=1x1x128 pad=0_0x0_0x0_127}, to_apply=%region_5.5 | reduce-window | flops 8323072 | bytes 524292 | tf_op jit(solution)/shard_map/while/body/eval_jaxpr/reduce_window_sum | solution.py:33
  233.6 0.4 fusion.67
  234.0 2.4 convolution_convert_fusion.2
  236.4 41.1 %reduce-scatter.5.cloned.1.call-done = bf16[256,2048]{1,0:T(8,128)(2,1)} async-done(((bf16[2048,2048]{1,0:T(8,128)(2,1)}), bf16[256,2048]{1,0:T(8,128)(2,1)}) %reduce-scatter.5.cloned.1.call-update) | async-done | bytes 1048592 | tf_op jit(solution)/shard_map/reduce_scatter | solution.py:138
  277.5 3.6 %all-to-all-start.1 = ((bf16[4,64,2048]{2,1,0:T(8,128)(2,1)}), bf16[4,64,2048]{2,1,0:T(8,128)(2,1)S(1)}, u32[]{:S(2)}, u32[]{:S(2)}) async-start(bf16[4,64,2048]{2,1,0:T(8,128)(2,1)} %bitcast.86), calls=%async_computation.3 | async-start | bytes 2097152 | tf_op jit(solution)/shard_map/all_to_all | solution.py:144
  281.5 11.6 %all-to-all-done.1 = bf16[4,64,2048]{2,1,0:T(8,128)(2,1)S(1)} async-done(((bf16[4,64,2048]{2,1,0:T(8,128)(2,1)}), bf16[4,64,2048]{2,1,0:T(8,128)(2,1)S(1)}, u32[]{:S(2)}, u32[]{:S(2)}) %all-to-all-start.1) | async-done | bytes 1048608 | tf_op jit(solution)/shard_map/all_to_all | solution.py:144
  293.1 1.3 fusion.21
  294.4 15.9 %reduce-scatter.3.cloned.1.call-done = bf16[16,2048]{1,0:T(8,128)(2,1)} async-done(((bf16[128,2048]{1,0:T(8,128)(2,1)}), bf16[16,2048]{1,0:T(8,128)(2,1)}) %reduce-scatter.3.cloned.1.call-update) | async-done | bytes 65552 | tf_op jit(solution)/shard_map/reduce_scatter | solution.py:42
  (96 shorter events, 2.1 us)
Async XLA Ops:
  7.2 169.6 %copy-start = (bf16[1,448,2048]{2,1,0:T(8,128)(2,1)S(1)}, bf16[1,448,2048]{2,1,0:T(8,128)(2,1)}, u32[]{:S(2)}) copy-start(bf16[1,448,2048]{2,1,0:T(8,128)(2,1)} %param.29) | copy-start | bytes 5505028
  7.2 270.4 %reduce-scatter.5.cloned.1.call-start = ((), (), s32[]{:S(2)}) async-start(), calls=%async_computation.5 | async-start | bytes 9437184 | tf_op jit(solution)/shard_map/reduce_scatter | solution.py:138
  35.3 16.0 %collective-permute-start.2 = (bf16[256,2048]{1,0:T(8,128)(2,1)S(1)}, bf16[256,2048]{1,0:T(8,128)(2,1)S(1)}, u32[]{:S(2)}, u32[]{:S(2)}) collective-permute-start(bf16[256,2048]{1,0:T(8,128)(2,1)S(1)} %bitcast.80), channel_id=1, source_target_pairs={{0,1},{1,2},{2,3},{3,4},{4,5},{5,6},{6,7},{7,0},{8,9},{9,10},{10,1... | collective-permute-start | bytes 3145736 | tf_op jit(solution)/shard_map/ppermute | solution.py:128
  51.4 1.0 copy-start.1
  52.4 16.0 %collective-permute-start.3 = (bf16[256,2048]{1,0:T(8,128)(2,1)S(1)}, bf16[256,2048]{1,0:T(8,128)(2,1)S(1)}, u32[]{:S(2)}, u32[]{:S(2)}) collective-permute-start(bf16[256,2048]{1,0:T(8,128)(2,1)S(1)} %collective-permute-done.2), channel_id=1, source_target_pairs={{0,1},{1,2},{2,3},{3,4},{4,5},{5,6},{6,7},{7,0},{8,9},{9,10},{10,1... | collective-permute-start | bytes 3145736 | tf_op jit(solution)/shard_map/ppermute | solution.py:128
  68.4 1.0 copy-start.3
  69.4 16.0 %collective-permute-start.4 = (bf16[256,2048]{1,0:T(8,128)(2,1)S(1)}, bf16[256,2048]{1,0:T(8,128)(2,1)S(1)}, u32[]{:S(2)}, u32[]{:S(2)}) collective-permute-start(bf16[256,2048]{1,0:T(8,128)(2,1)S(1)} %collective-permute-done.3), channel_id=1, source_target_pairs={{0,1},{1,2},{2,3},{3,4},{4,5},{5,6},{6,7},{7,0},{8,9},{9,10},{10,1... | collective-permute-start | bytes 3145736 | tf_op jit(solution)/shard_map/ppermute | solution.py:128
  85.4 1.0 copy-start.5
  86.4 16.0 %collective-permute-start.5 = (bf16[256,2048]{1,0:T(8,128)(2,1)S(1)}, bf16[256,2048]{1,0:T(8,128)(2,1)S(1)}, u32[]{:S(2)}, u32[]{:S(2)}) collective-permute-start(bf16[256,2048]{1,0:T(8,128)(2,1)S(1)} %collective-permute-done.4), channel_id=1, source_target_pairs={{0,1},{1,2},{2,3},{3,4},{4,5},{5,6},{6,7},{7,0},{8,9},{9,10},{10,1... | collective-permute-start | bytes 3145736 | tf_op jit(solution)/shard_map/ppermute | solution.py:128
  102.4 1.0 copy-start.7
  103.4 16.0 %collective-permute-start.6 = (bf16[256,2048]{1,0:T(8,128)(2,1)S(1)}, bf16[256,2048]{1,0:T(8,128)(2,1)S(1)}, u32[]{:S(2)}, u32[]{:S(2)}) collective-permute-start(bf16[256,2048]{1,0:T(8,128)(2,1)S(1)} %collective-permute-done.5), channel_id=1, source_target_pairs={{0,1},{1,2},{2,3},{3,4},{4,5},{5,6},{6,7},{7,0},{8,9},{9,10},{10,1... | collective-permute-start | bytes 3145736 | tf_op jit(solution)/shard_map/ppermute | solution.py:128
  119.5 1.0 copy-start.9
  120.4 16.1 %collective-permute-start.7 = (bf16[256,2048]{1,0:T(8,128)(2,1)S(1)}, bf16[256,2048]{1,0:T(8,128)(2,1)}, u32[]{:S(2)}, u32[]{:S(2)}) collective-permute-start(bf16[256,2048]{1,0:T(8,128)(2,1)S(1)} %collective-permute-done.6), channel_id=1, source_target_pairs={{0,1},{1,2},{2,3},{3,4},{4,5},{5,6},{6,7},{7,0},{8,9},{9,10},{10,1... | collective-permute-start | bytes 3145736 | tf_op jit(solution)/shard_map/ppermute | solution.py:128
  136.6 16.3 %collective-permute-start.8 = (bf16[256,2048]{1,0:T(8,128)(2,1)}, bf16[256,2048]{1,0:T(8,128)(2,1)}, u32[]{:S(2)}, u32[]{:S(2)}) collective-permute-start(bf16[256,2048]{1,0:T(8,128)(2,1)} %collective-permute-done.7), channel_id=1, source_target_pairs={{0,1},{1,2},{2,3},{3,4},{4,5},{5,6},{6,7},{7,0},{8,9},{9,10},{10,1... | collective-permute-start | bytes 3145736 | tf_op jit(solution)/shard_map/ppermute | solution.py:128
  136.6 28.1 %copy-start.10 = (bf16[256,2048]{1,0:T(8,128)(2,1)S(1)}, bf16[256,2048]{1,0:T(8,128)(2,1)}, u32[]{:S(2)}) copy-start(bf16[256,2048]{1,0:T(8,128)(2,1)} %copy-done.9) | copy-start | bytes 3145732
  136.6 28.2 %copy-start.8 = (bf16[256,2048]{1,0:T(8,128)(2,1)S(1)}, bf16[256,2048]{1,0:T(8,128)(2,1)}, u32[]{:S(2)}) copy-start(bf16[256,2048]{1,0:T(8,128)(2,1)} %copy-done.7) | copy-start | bytes 3145732
  136.6 28.3 %copy-start.6 = (bf16[256,2048]{1,0:T(8,128)(2,1)S(1)}, bf16[256,2048]{1,0:T(8,128)(2,1)}, u32[]{:S(2)}) copy-start(bf16[256,2048]{1,0:T(8,128)(2,1)} %copy-done.5) | copy-start | bytes 3145732
  136.6 28.4 %copy-start.4 = (bf16[256,2048]{1,0:T(8,128)(2,1)S(1)}, bf16[256,2048]{1,0:T(8,128)(2,1)}, u32[]{:S(2)}) copy-start(bf16[256,2048]{1,0:T(8,128)(2,1)} %copy-done.3) | copy-start | bytes 3145732
  136.6 28.4 %copy-start.2 = (bf16[256,2048]{1,0:T(8,128)(2,1)S(1)}, bf16[256,2048]{1,0:T(8,128)(2,1)}, u32[]{:S(2)}) copy-start(bf16[256,2048]{1,0:T(8,128)(2,1)} %copy-done.1) | copy-start | bytes 3145732
  136.6 34.3 %copy-start.19 = (bf16[1,2048,448]{1,2,0:T(8,128)(2,1)S(1)}, bf16[1,2048,448]{1,2,0:T(8,128)(2,1)}, u32[]{:S(2)}) copy-start(bf16[1,2048,448]{1,2,0:T(8,128)(2,1)} %param.28) | copy-start | bytes 5505028
  165.2 5.7 %copy-start.12 = (bf16[4096,2048]{1,0:T(8,128)(2,1)}, bf16[4096,2048]{1,0:T(8,128)(2,1)S(1)}, u32[]{:S(2)}) copy-start(bf16[4096,2048]{1,0:T(8,128)(2,1)S(1)} %constant_dynamic-update-slice_fusion) | copy-start | bytes 50331652
  176.8 14.7 %copy-start.11 = (bf16[128,256]{1,0:T(8,128)(2,1)S(1)}, bf16[128,256]{1,0:T(8,128)(2,1)}, u32[]{:S(2)}) copy-start(bf16[128,256]{1,0:T(8,128)(2,1)} %param.16) | copy-start | bytes 196612
  176.8 14.8 %copy-start.13 = (bf16[128,256]{1,0:T(8,128)(2,1)S(1)}, bf16[128,256]{1,0:T(8,128)(2,1)}, u32[]{:S(2)}) copy-start(bf16[128,256]{1,0:T(8,128)(2,1)} %param.17) | copy-start | bytes 196612
  176.8 14.9 %copy-start.14 = (bf16[128,256]{1,0:T(8,128)(2,1)S(1)}, bf16[128,256]{1,0:T(8,128)(2,1)}, u32[]{:S(2)}) copy-start(bf16[128,256]{1,0:T(8,128)(2,1)} %param.18) | copy-start | bytes 196612
  176.8 15.0 %copy-start.18 = (f32[64]{0:T(128)S(1)}, f32[64]{0:T(128)}, u32[]{:S(2)}) copy-start(f32[64]{0:T(128)} %param.20) | copy-start | bytes 772
  176.8 15.3 %copy-start.17 = (f32[64]{0:T(128)S(1)}, f32[64]{0:T(128)}, u32[]{:S(2)}) copy-start(f32[64]{0:T(128)} %param.19) | copy-start | bytes 772
  176.8 15.4 %copy-start.20 = (f32[4]{0:T(128)S(1)}, f32[4]{0:T(128)}, u32[]{:S(2)}) copy-start(f32[4]{0:T(128)} %param.21) | copy-start | bytes 52
  191.1 90.2 %copy-start.16 = (f32[128,2]{0,1:T(2,128)S(1)}, f32[128,2]{0,1:T(2,128)}, u32[]{:S(2)}) copy-start(f32[128,2]{0,1:T(2,128)} %param.26) | copy-start | bytes 3076
  191.1 90.3 %copy-start.15 = (s32[128,2]{0,1:T(2,128)S(1)}, s32[128,2]{0,1:T(2,128)}, u32[]{:S(2)}) copy-start(s32[128,2]{0,1:T(2,128)} %param.25) | copy-start | bytes 3076
  191.2 119.1 %reduce-scatter.3.cloned.1.call-start = ((), (), s32[]{:S(2)}) async-start(), calls=%async_computation.4 | async-start | bytes 589824 | tf_op jit(solution)/shard_map/reduce_scatter | solution.py:42
  197.6 6.2 %collective-permute-start = (bf16[128,256]{0,1:T(8,128)(2,1)S(1)}, bf16[128,256]{0,1:T(8,128)(2,1)S(1)}, u32[]{:S(2)}, u32[]{:S(2)}) collective-permute-start(bf16[128,256]{0,1:T(8,128)(2,1)S(1)} %get-tuple-element.268), channel_id=1, source_target_pairs={{0,8},{8,16},{16,24},{1,9},{9,17},{17,25},{2,10},{10,18},{18,26},{... | collective-permute-start | bytes 196616 | tf_op jit(solution)/shard_map/while/body/eval_jaxpr/ppermute | solution.py:14
  200.4 8.3 %collective-permute-start.1 = (bf16[128,256]{0,1:T(8,128)(2,1)S(1)}, bf16[128,256]{0,1:T(8,128)(2,1)S(1)}, u32[]{:S(2)}, u32[]{:S(2)}) collective-permute-start(bf16[128,256]{0,1:T(8,128)(2,1)S(1)} %get-tuple-element.269), channel_id=1, source_target_pairs={{0,8},{8,16},{16,24},{1,9},{9,17},{17,25},{2,10},{10,18},{18,26},{... | collective-permute-start | bytes 196616 | tf_op jit(solution)/shard_map/while/body/eval_jaxpr/ppermute | solution.py:14
  209.2 7.0 %collective-permute-start = (bf16[128,256]{0,1:T(8,128)(2,1)S(1)}, bf16[128,256]{0,1:T(8,128)(2,1)S(1)}, u32[]{:S(2)}, u32[]{:S(2)}) collective-permute-start(bf16[128,256]{0,1:T(8,128)(2,1)S(1)} %get-tuple-element.268), channel_id=1, source_target_pairs={{0,8},{8,16},{16,24},{1,9},{9,17},{17,25},{2,10},{10,18},{18,26},{... | collective-permute-start | bytes 196616 | tf_op jit(solution)/shard_map/while/body/eval_jaxpr/ppermute | solution.py:14
  212.6 8.6 %collective-permute-start.1 = (bf16[128,256]{0,1:T(8,128)(2,1)S(1)}, bf16[128,256]{0,1:T(8,128)(2,1)S(1)}, u32[]{:S(2)}, u32[]{:S(2)}) collective-permute-start(bf16[128,256]{0,1:T(8,128)(2,1)S(1)} %get-tuple-element.269), channel_id=1, source_target_pairs={{0,8},{8,16},{16,24},{1,9},{9,17},{17,25},{2,10},{10,18},{18,26},{... | collective-permute-start | bytes 196616 | tf_op jit(solution)/shard_map/while/body/eval_jaxpr/ppermute | solution.py:14
  221.6 7.0 %collective-permute-start = (bf16[128,256]{0,1:T(8,128)(2,1)S(1)}, bf16[128,256]{0,1:T(8,128)(2,1)S(1)}, u32[]{:S(2)}, u32[]{:S(2)}) collective-permute-start(bf16[128,256]{0,1:T(8,128)(2,1)S(1)} %get-tuple-element.268), channel_id=1, source_target_pairs={{0,8},{8,16},{16,24},{1,9},{9,17},{17,25},{2,10},{10,18},{18,26},{... | collective-permute-start | bytes 196616 | tf_op jit(solution)/shard_map/while/body/eval_jaxpr/ppermute | solution.py:14
  224.3 9.2 %collective-permute-start.1 = (bf16[128,256]{0,1:T(8,128)(2,1)S(1)}, bf16[128,256]{0,1:T(8,128)(2,1)S(1)}, u32[]{:S(2)}, u32[]{:S(2)}) collective-permute-start(bf16[128,256]{0,1:T(8,128)(2,1)S(1)} %get-tuple-element.269), channel_id=1, source_target_pairs={{0,8},{8,16},{16,24},{1,9},{9,17},{17,25},{2,10},{10,18},{18,26},{... | collective-permute-start | bytes 196616 | tf_op jit(solution)/shard_map/while/body/eval_jaxpr/ppermute | solution.py:14
  277.5 15.5 %all-to-all-start.1 = ((bf16[4,64,2048]{2,1,0:T(8,128)(2,1)}), bf16[4,64,2048]{2,1,0:T(8,128)(2,1)S(1)}, u32[]{:S(2)}, u32[]{:S(2)}) async-start(bf16[4,64,2048]{2,1,0:T(8,128)(2,1)} %bitcast.86), calls=%async_computation.3 | async-start | bytes 2097152 | tf_op jit(solution)/shard_map/all_to_all | solution.py:144
Sparse Core Ops, SparseCore 0:
  191.3 86.2 reduce-scatter.4
  280.4 29.8 reduce-scatter.2
